TPU v7x, 32 devices: a whole 2x2x4 slice. The times are simulated.
32 devices in a mesh: sp: 8 (over z, y), tp: 4 (over x, core).
Axes of the slice: x: 2, y: 2, z: 4, core: 2. Of those that a mesh axis runs over, the one named last changes fastest.
Arguments:
- queries: bfloat16 [6144, 1536], P('sp', 'tp'), may hold values from -130 to 130, as said below
- keys: bfloat16 [6144, 512], P('sp', 'tp'), may hold values from -6 to 6
- values: bfloat16 [6144, 512], P('sp', 'tp'), may hold values from -6 to 6
- residual: bfloat16 [6144, 2048], P(('sp', 'tp')), may hold values from -6 to 6
- sinks: float32 [12], P('tp'), may hold values from 2 to 6
- out_weight: bfloat16 [1536, 2048], P('tp'), may hold values from -0.15625 to 0.15625
- up_weight: bfloat16 [2048, 8192], P('sp', 'tp'), may hold values from -0.125 to 0.125
- down_weight: bfloat16 [8192, 2048], P('tp', 'sp'), may hold values from -0.0625 to 0.0625
- gains: float32 [2, 2048], replicated, may hold values from 0.1 to 1.9
- biases: float32 [2, 2048], replicated, may hold values from -3 to 3
Outputs:
- layer_out: bfloat16 [6144, 2048], P(('sp', 'tp'))
Inputs may be any that keep to these rules, and one draw needn't show every extreme that they name: `queries`: entries of order one, with some rows far larger in some draws.
All inputs are finite; a program needn't handle non-finite values.
Results may differ from a plain program's by a relative error of at most 0.0095.
Values may be sent and summed in bfloat16 or wider, within the bound.
A program may use at most 128 MiB of HBM per device.

v0:
```python
import jax
import jax.numpy as jnp
from jax import lax
from jax.sharding import PartitionSpec as P

HEADS = 12
HEAD = 128
WINDOW = 128
deep_alpha = 1.6817928
norm_eps = 1e-05
neg_big = -1e30


def from_behind(block, axis, distance):
    devices = range(lax.axis_size(axis))
    route = [(i - distance, i) for i in devices if i - distance in devices]
    return lax.ppermute(block, axis, route)


def layer_norm(stream, gain, bias):
    mean = jnp.mean(stream, axis=-1, keepdims=True)
    spread = jnp.mean(jnp.square(stream - mean), axis=-1, keepdims=True)
    return ((stream - mean) * lax.rsqrt(spread + norm_eps) * gain + bias).astype(jnp.bfloat16)


def attend(queries, keys, values, before, sinks, offset, rank_tp):
    tokens = keys.shape[0]
    kv_local = keys.shape[1] // HEAD
    heads_local = sinks.shape[0]
    group = heads_local // kv_local
    blocks = tokens // WINDOW
    q_blocks = queries.reshape(blocks, WINDOW, kv_local, group, HEAD)
    key_ext = jnp.concatenate([before[0], keys], axis=0).reshape(tokens + WINDOW, kv_local, HEAD)
    val_ext = jnp.concatenate([before[1], values], axis=0).reshape(tokens + WINDOW, kv_local, HEAD)
    key_win = jnp.concatenate(
        [
            key_ext[:tokens].reshape(blocks, WINDOW, kv_local, HEAD),
            key_ext[WINDOW:].reshape(blocks, WINDOW, kv_local, HEAD),
        ],
        axis=1,
    )
    val_win = jnp.concatenate(
        [
            val_ext[:tokens].reshape(blocks, WINDOW, kv_local, HEAD),
            val_ext[WINDOW:].reshape(blocks, WINDOW, kv_local, HEAD),
        ],
        axis=1,
    )
    logits = jnp.einsum(
        "nqkgd,nskd->nkgqs", q_blocks, key_win, preferred_element_type=jnp.float32
    ) * HEAD ** (-0.5)
    q_index = jnp.arange(WINDOW, dtype=jnp.int32)[:, None]
    k_index = jnp.arange(2 * WINDOW, dtype=jnp.int32)[None, :]
    dist = q_index + WINDOW - k_index
    block_id = jnp.arange(blocks, dtype=jnp.int32)[:, None, None]
    key_pos = offset + block_id * WINDOW - WINDOW + k_index
    valid = (dist >= 0) & (dist < WINDOW) & (key_pos >= 0)
    heads = (jnp.arange(heads_local, dtype=jnp.int32) + rank_tp * heads_local).astype(jnp.float32)
    slopes = jnp.exp2(-8.0 * (heads + 1.0) / HEADS).reshape(kv_local, group)[:, :, None, None]
    logits = logits - slopes * dist.astype(jnp.float32)
    logits = jnp.where(valid[:, None, None], logits, neg_big)
    sink = sinks.reshape(kv_local, group)[:, :, None, None]
    top = jnp.maximum(jnp.max(logits, axis=-1, keepdims=True), sink)
    probs = jnp.exp(logits - top)
    denom = jnp.sum(probs, axis=-1, keepdims=True) + jnp.exp(sink - top)
    weight = (probs / denom).astype(jnp.bfloat16)
    attended = jnp.einsum("nkgqs,nskd->nqkgd", weight, val_win, preferred_element_type=jnp.float32)
    return attended.astype(jnp.bfloat16).reshape(tokens, heads_local * HEAD)


def on_device(
    queries, keys, values, residual, sinks, out_weight, up_weight, down_weight, gains, biases
):
    tokens = queries.shape[0]
    rank_tp = lax.axis_index("tp")
    up_full, down_full = (
        lax.all_gather(up_weight, "sp", axis=0, tiled=True),
        lax.all_gather(down_weight, "sp", axis=1, tiled=True),
    )
    tails = jnp.stack([keys[tokens - WINDOW :], values[tokens - WINDOW :]])
    before = from_behind(tails, "sp", 1)
    offset = lax.axis_index("sp") * tokens
    attended = attend(queries, keys, values, before, sinks, offset, rank_tp)
    mix = lax.psum_scatter(
        jnp.dot(attended, out_weight, preferred_element_type=jnp.float32).astype(jnp.bfloat16),
        "tp",
        scatter_dimension=0,
        tiled=True,
    ).astype(jnp.float32)
    normed = layer_norm(deep_alpha * residual.astype(jnp.float32) + mix, gains[0], biases[0])
    whole = lax.all_gather(normed, "tp", axis=0, tiled=True)
    upward = jnp.dot(whole, up_full, preferred_element_type=jnp.float32)
    act = jnp.square(jax.nn.relu(upward)).astype(jnp.bfloat16)
    terms = jnp.dot(act, down_full, preferred_element_type=jnp.float32)
    ffn = lax.psum_scatter(
        terms.astype(jnp.bfloat16), "tp", scatter_dimension=0, tiled=True
    ).astype(jnp.float32)
    return layer_norm(deep_alpha * normed.astype(jnp.float32) + ffn, gains[1], biases[1])


def solution(mesh):
    return jax.shard_map(
        on_device,
        mesh=mesh,
        in_specs=(
            P("sp", "tp"),
            P("sp", "tp"),
            P("sp", "tp"),
            P(("sp", "tp"), None),
            P("tp"),
            P("tp", None),
            P("sp", "tp"),
            P("tp", "sp"),
            P(),
            P(),
        ),
        out_specs=P(("sp", "tp"), None),
        check_vma=False,
    )
```

profile of v0, /device:TPU:0, one launch (start us, length us, event | category | flops | bytes accessed | tf_op | source)
XLA Modules:
  0.0 408.7 jit_solution(9440139312392734191)
XLA Ops:
  6.5 0.9 slice_bitcast_fusion.2
  7.5 0.6 pad_maximum_fusion.2
  8.1 5.5 %collective-permute-start = (bf16[2,128,128]{2,1,0:T(8,128)(2,1)}, bf16[2,128,128]{2,1,0:T(8,128)(2,1)}, u32[]{:S(2)}, u32[]{:S(2)}) collective-permute-start(bf16[2,128,128]{2,1,0:T(8,128)(2,1)} %pad_maximum_fusion.2), channel_id=1, source_target_pairs={{0,4},{4,8},{8,12},{12,16},{16,20},{20,24},{24,28},{1,5},{5,9},{9,... | collective-permute-start | bytes 196616 | tf_op jit(solution)/shard_map/ppermute | solution.py:17
  13.9 1.0 broadcast_and_fusion
  14.9 0.2 reshape.206
  15.1 0.2 copy.14
  15.3 0.8 slice_bitcast_fusion.1
  16.1 0.9 pad_maximum_fusion
  17.0 1.7 fusion.21
  18.8 1.3 copy-done.5
  20.1 0.4 fusion.1
  20.5 0.2 copy.13
  20.7 2.2 fusion.2
  22.9 0.4 copy.18
  23.3 3.5 convolution_convert_fusion.1
  26.9 0.6 copy-done.8
  27.6 39.3 %reduce-scatter.3.cloned.1.call-done = bf16[192,2048]{1,0:T(8,128)(2,1)} async-done(((bf16[768,2048]{1,0:T(8,128)(2,1)}), bf16[192,2048]{1,0:T(8,128)(2,1)}) %reduce-scatter.3.cloned.1.call-update) | async-done | bytes 786448 | tf_op jit(solution)/shard_map/reduce_scatter | solution.py:84
  66.9 1.5 fusion.3
  68.5 0.4 multiply_reduce_fusion.1
  69.0 1.4 add_convert_fusion.1
  70.4 0.7 all-gather.6.cloned.1.call-update
  71.1 0.5 all-gather.8.cloned.1.call-update
  71.7 0.2 reduce-scatter.5.cloned.1.call-start
  71.9 27.1 %all-gather.4.cloned.1.call-done = bf16[768,2048]{1,0:T(8,128)(2,1)} async-done(((bf16[192,2048]{1,0:T(8,128)(2,1)}), bf16[768,2048]{1,0:T(8,128)(2,1)}) %all-gather.4.cloned.1.call-update) | async-done | bytes 3145744 | tf_op jit(solution)/shard_map/all_gather | solution.py:91
  99.0 126.6 %all-gather.6.cloned.1.call-done = bf16[2048,2048]{1,0:T(8,128)(2,1)} async-done(((bf16[256,2048]{1,0:T(8,128)(2,1)}), bf16[2048,2048]{1,0:T(8,128)(2,1)}) %all-gather.6.cloned.1.call-update) | async-done | bytes 8388624 | tf_op jit(solution)/shard_map/all_gather | solution.py:77
  225.6 11.9 %multiply_convert_fusion = bf16[768,2048]{1,0:T(8,128)(2,1)} fusion(bf16[768,2048]{1,0:T(8,128)(2,1)} %all-gather.4.cloned.1.call-done, bf16[2048,2048]{1,0:T(8,128)(2,1)} %all-gather.6.cloned.1.call-done), kind=kOutput, calls=%fused_computation | convolution fusion | flops 6447169536 | bytes 14680064 | tf_op jit(solution)/shard_map/dot_general | solution.py:92
  237.5 113.2 %all-gather.8.cloned.1.call-done = bf16[2048,2048]{1,0:T(8,128)(2,1)} async-done(((bf16[2048,256]{1,0:T(8,128)(2,1)}), bf16[2048,2048]{1,0:T(8,128)(2,1)}) %all-gather.8.cloned.1.call-update) | async-done | bytes 8388624 | tf_op jit(solution)/shard_map/all_gather | solution.py:78
  350.7 11.8 %convolution_convert_fusion = bf16[768,2048]{1,0:T(8,128)(2,1)} fusion(bf16[768,2048]{1,0:T(8,128)(2,1)} %multiply_convert_fusion, bf16[2048,2048]{1,0:T(8,128)(2,1)} %all-gather.8.cloned.1.call-done), kind=kOutput, calls=%fused_computation.1 | convolution fusion | flops 6444023808 | bytes 14680064 | tf_op jit(solution)/shard_map/dot_general | solution.py:94
  362.6 36.2 %reduce-scatter.5.cloned.1.call-done = bf16[192,2048]{1,0:T(8,128)(2,1)} async-done(((bf16[768,2048]{1,0:T(8,128)(2,1)}), bf16[192,2048]{1,0:T(8,128)(2,1)}) %reduce-scatter.5.cloned.1.call-update) | async-done | bytes 786448 | tf_op jit(solution)/shard_map/reduce_scatter | solution.py:95
  398.8 1.5 fusion.4
  400.3 0.4 multiply_reduce_fusion
  400.8 1.4 add_convert_fusion
  (44 shorter events, 0.7 us)
Async XLA Ops:
  6.5 16.8 %copy-start = (bf16[384,2048]{1,0:T(8,128)(2,1)S(1)}, bf16[384,2048]{1,0:T(8,128)(2,1)}, u32[]{:S(2)}) copy-start(bf16[384,2048]{1,0:T(8,128)(2,1)} %param.15) | copy-start | bytes 4718596
  6.5 8.5 %copy-start.6 = (bf16[768,128]{1,0:T(8,128)(2,1)S(1)}, bf16[768,128]{1,0:T(8,128)(2,1)}, u32[]{:S(2)}) copy-start(bf16[768,128]{1,0:T(8,128)(2,1)} %param.12) | copy-start | bytes 589828
  6.5 8.3 %copy-start.7 = (bf16[768,384]{1,0:T(8,128)(2,1)S(1)}, bf16[768,384]{1,0:T(8,128)(2,1)}, u32[]{:S(2)}) copy-start(bf16[768,384]{1,0:T(8,128)(2,1)} %param.10) | copy-start | bytes 1769476
  6.5 60.4 %reduce-scatter.3.cloned.1.call-start = ((), (), s32[]{:S(2)}) async-start(), calls=%async_computation.2 | async-start | bytes 3932160 | tf_op jit(solution)/shard_map/reduce_scatter | solution.py:84
  8.1 7.1 %collective-permute-start = (bf16[2,128,128]{2,1,0:T(8,128)(2,1)}, bf16[2,128,128]{2,1,0:T(8,128)(2,1)}, u32[]{:S(2)}, u32[]{:S(2)}) collective-permute-start(bf16[2,128,128]{2,1,0:T(8,128)(2,1)} %pad_maximum_fusion.2), channel_id=1, source_target_pairs={{0,4},{4,8},{8,12},{12,16},{16,20},{20,24},{24,28},{1,5},{5,9},{9,... | collective-permute-start | bytes 196616 | tf_op jit(solution)/shard_map/ppermute | solution.py:17
  17.0 1.7 copy-start.10
  18.7 1.4 copy-start.5
  26.8 0.7 copy-start.8
  26.8 0.7 copy-start.9
  26.8 40.1 %copy-start.2 = (bf16[192,2048]{1,0:T(8,128)(2,1)S(1)}, bf16[192,2048]{1,0:T(8,128)(2,1)}, u32[]{:S(2)}) copy-start(bf16[192,2048]{1,0:T(8,128)(2,1)} %param.13) | copy-start | bytes 2359300
  26.9 72.1 %all-gather.4.cloned.1.call-start = ((), (), s32[]{:S(2)}) async-start(), calls=%async_computation.3 | async-start | bytes 3932160 | tf_op jit(solution)/shard_map/all_gather | solution.py:91
  66.9 1.6 copy-start.3
  70.3 155.3 %all-gather.6.cloned.1.call-start = ((), (), s32[]{:S(2)}) async-start(), calls=%async_computation.4 | async-start | bytes 9437184 | tf_op jit(solution)/shard_map/all_gather | solution.py:77
  71.1 279.6 %all-gather.8.cloned.1.call-start = ((), (), s32[]{:S(2)}) async-start(), calls=%async_computation.5 | async-start | bytes 9437184 | tf_op jit(solution)/shard_map/all_gather | solution.py:78
  71.7 327.1 %reduce-scatter.5.cloned.1.call-start = ((), (), s32[]{:S(2)}) async-start(), calls=%async_computation.6 | async-start | bytes 3932160 | tf_op jit(solution)/shard_map/reduce_scatter | solution.py:95
  362.5 36.2 %copy-start.1 = (bf16[192,2048]{1,0:T(8,128)(2,1)S(1)}, bf16[192,2048]{1,0:T(8,128)(2,1)}, u32[]{:S(2)}) copy-start(bf16[192,2048]{1,0:T(8,128)(2,1)} %add_convert_fusion.1) | copy-start | bytes 2359300
  398.8 1.6 copy-start.4
Sparse Core Ops, SparseCore 0:
  27.0 39.9 reduce-scatter.2
  70.5 28.4 all-gather.3
  101.1 124.4 all-gather.5
  227.5 123.1 all-gather.7
  362.7 36.0 reduce-scatter.4
where the time goes:
time: 409 us
  waiting for transfers between devices  344 us (84%)
  matrix products  31.1 us (8%)
  between operations  13.3 us (3%)
  other arithmetic  10 us (2%)
  starting transfers between devices  5.86 us (1%)
  local copies, waits for them, and re-layouts  4.69 us (1%)
    all_gather x1, waiting for transfers between devices, on_device(): lax.all_gather(up_weight, 'sp', axis=0, tiled=True)  127 us
    all_gather x1, waiting for transfers between devices, on_device(): lax.all_gather(down_weight, 'sp', axis=1, tiled=True)  113 us
    reduce_scatter x1, waiting for transfers between devices, on_device(): lax.psum_scatter(jnp.dot(attended, out_weight, preferred_element_type=jnp...  39.3 us
    reduce_scatter x1, waiting for transfers between devices, on_device(): lax.psum_scatter(terms.astype(jnp.bfloat16), 'tp', scatter_dimension=0, t...  36.2 us
    all_gather x1, waiting for transfers between devices, on_device(): whole = lax.all_gather(normed, 'tp', axis=0, tiled=True)  27.1 us
    dot_general x1, matrix products, on_device(): upward = jnp.dot(whole, up_full, preferred_element_type=jnp.float32)  11.9 us
    dot_general x1, matrix products, on_device(): terms = jnp.dot(act, down_full, preferred_element_type=jnp.float32)  11.8 us
  transfers between devices with their start and end apart: 6, of which 5 were waited for; matrix products, arithmetic and copies ran while one was open for 3% of the time, Pallas kernels for 0%

commit v1 on v0

--- a/solution.py
+++ b/solution.py
@@ -75,7 +75,7 @@
     rank_tp = lax.axis_index("tp")
     up_full, down_full = (
         lax.all_gather(up_weight, "sp", axis=0, tiled=True),
-        lax.all_gather(down_weight, "sp", axis=1, tiled=True),
+        jnp.concatenate(lax.all_gather(down_weight, "sp"), axis=1),
     )
     tails = jnp.stack([keys[tokens - WINDOW :], values[tokens - WINDOW :]])
     before = from_behind(tails, "sp", 1)

time: 409 us -> 377 us (0.922)
  waiting for transfers between devices: 344 us -> 304 us
  local copies, waits for them, and re-layouts: 4.69 us -> 15.9 us
  matrix products: 31.1 us -> 25.7 us
    all_gather x1, waiting for transfers between devices: 113 us -> 84.6 us  [on_device(): lax.all_gather(down_weight, 'sp')]
    reshape x0 -> x1, local copies, waits for them, and re-layouts: none -> 11.8 us  [on_device(): jnp.concatenate(lax.all_gather(down_weight, 'sp'), axis=1)]
    all_gather x1, waiting for transfers between devices: 27.1 us -> 16.2 us  [on_device(): whole = lax.all_gather(normed, 'tp', axis=0, tiled=True)]
  transfers between devices with their start and end apart: 6 -> 6, of which waited for: 5 -> 5; matrix products, arithmetic and copies ran while one was open for 3% -> 4% of each run, Pallas kernels for 0% -> 0%
where the time goes in v1:
time: 377 us; the launch traced here: 376 us
  waiting for transfers between devices  304 us (81%)
  matrix products  25.7 us (7%)
  local copies, waits for them, and re-layouts  15.9 us (4%)
  between operations  15.2 us (4%)
  other arithmetic  9.99 us (3%)
  starting transfers between devices  5.87 us (2%)
    all_gather x1, waiting for transfers between devices, on_device(): lax.all_gather(up_weight, 'sp', axis=0, tiled=True)  126 us
    all_gather x1, waiting for transfers between devices, on_device(): lax.all_gather(down_weight, 'sp')  84.6 us
    reduce_scatter x1, waiting for transfers between devices, on_device(): lax.psum_scatter(jnp.dot(attended, out_weight, preferred_element_type=jnp...  39.3 us
    reduce_scatter x1, waiting for transfers between devices, on_device(): lax.psum_scatter(terms.astype(jnp.bfloat16), 'tp', scatter_dimension=0, t...  36.2 us
    all_gather x1, waiting for transfers between devices, on_device(): whole = lax.all_gather(normed, 'tp', axis=0, tiled=True)  16.2 us
    reshape x1, local copies, waits for them, and re-layouts, on_device(): jnp.concatenate(lax.all_gather(down_weight, 'sp'), axis=1)  11.8 us
    dot_general x1, matrix products, on_device(): upward = jnp.dot(whole, up_full, preferred_element_type=jnp.float32)  10.2 us
    dot_general x1, matrix products, on_device(): terms = jnp.dot(act, down_full, preferred_element_type=jnp.float32)  8.14 us
  transfers between devices with their start and end apart: 6, of which 5 were waited for; matrix products, arithmetic and copies ran while one was open for 4% of the time, Pallas kernels for 0%

profile of v1, /device:TPU:0, one launch (start us, length us, event | category | flops | bytes accessed | tf_op | source)
XLA Modules:
  0.0 376.3 jit_solution(1970613990248192173)
XLA Ops:
  7.4 0.9 slice_bitcast_fusion.2
  8.3 0.6 pad_maximum_fusion.2
  8.9 5.5 %collective-permute-start = (bf16[2,128,128]{2,1,0:T(8,128)(2,1)}, bf16[2,128,128]{2,1,0:T(8,128)(2,1)}, u32[]{:S(2)}, u32[]{:S(2)}) collective-permute-start(bf16[2,128,128]{2,1,0:T(8,128)(2,1)} %pad_maximum_fusion.2), channel_id=1, source_target_pairs={{0,4},{4,8},{8,12},{12,16},{16,20},{20,24},{24,28},{1,5},{5,9},{9,... | collective-permute-start | bytes 196616 | tf_op jit(solution)/shard_map/ppermute | solution.py:17
  14.7 1.0 broadcast_and_fusion
  15.7 0.2 reshape.215
  15.9 0.2 copy.20
  16.1 0.8 slice_bitcast_fusion.1
  16.9 0.9 pad_maximum_fusion
  17.8 1.7 fusion.21
  19.6 1.3 copy-done.6
  20.9 0.4 fusion.1
  21.4 0.2 copy.19
  21.5 2.2 fusion.2
  23.7 0.4 copy.24
  24.2 3.6 convolution_convert_fusion.1
  27.8 0.5 all-gather.9.cloned.1.call-update
  28.5 39.3 %reduce-scatter.3.cloned.1.call-done = bf16[192,2048]{1,0:T(8,128)(2,1)} async-done(((bf16[768,2048]{1,0:T(8,128)(2,1)}), bf16[192,2048]{1,0:T(8,128)(2,1)}) %reduce-scatter.3.cloned.1.call-update) | async-done | bytes 786448 | tf_op jit(solution)/shard_map/reduce_scatter | solution.py:84
  67.8 1.5 fusion.3
  69.4 0.4 multiply_reduce_fusion.1
  69.9 1.4 add_convert_fusion.1
  71.3 0.5 all-gather.7.cloned.1.call-update
  71.8 0.2 reduce-scatter.5.cloned.1.call-start
  72.0 84.6 %all-gather.9.cloned.1.call-done = bf16[16384,256]{1,0:T(8,128)(2,1)} async-done(((bf16[2048,256]{1,0:T(8,128)(2,1)}), bf16[16384,256]{1,0:T(8,128)(2,1)}) %all-gather.9.cloned.1.call-update) | async-done | bytes 8388624 | tf_op jit(solution)/shard_map/all_gather | solution.py:78
  156.6 11.8 %copy.25 = bf16[2048,8,256]{0,2,1:T(8,128)(2,1)} copy(bf16[2048,8,256]{2,0,1:T(8,128)(2,1)} %bitcast.59) | data formatting | bytes 16777216 | tf_op jit(solution)/shard_map/reshape | solution.py:78
  168.4 16.2 %all-gather.5.cloned.1.call-done = bf16[768,2048]{1,0:T(8,128)(2,1)} async-done(((bf16[192,2048]{1,0:T(8,128)(2,1)}), bf16[768,2048]{1,0:T(8,128)(2,1)}) %all-gather.5.cloned.1.call-update) | async-done | bytes 3145744 | tf_op jit(solution)/shard_map/all_gather | solution.py:91
  184.6 126.2 %all-gather.7.cloned.1.call-done = bf16[2048,2048]{1,0:T(8,128)(2,1)} async-done(((bf16[256,2048]{1,0:T(8,128)(2,1)}), bf16[2048,2048]{1,0:T(8,128)(2,1)}) %all-gather.7.cloned.1.call-update) | async-done | bytes 8388624 | tf_op jit(solution)/shard_map/all_gather | solution.py:77
  310.8 10.2 %multiply_convert_fusion = bf16[768,2048]{1,0:T(8,128)(2,1)S(1)} fusion(bf16[768,2048]{1,0:T(8,128)(2,1)} %all-gather.5.cloned.1.call-done, bf16[2048,2048]{1,0:T(8,128)(2,1)} %all-gather.7.cloned.1.call-done), kind=kOutput, calls=%fused_computation | convolution fusion | flops 6447169536 | bytes 14680064 | tf_op jit(solution)/shard_map/dot_general | solution.py:92
  321.0 8.1 %convolution_convert_fusion = bf16[768,2048]{1,0:T(8,128)(2,1)} fusion(bf16[768,2048]{1,0:T(8,128)(2,1)S(1)} %multiply_convert_fusion, bf16[2048,2048]{0,1:T(8,128)(2,1)S(1)} %bitcast.60), kind=kOutput, calls=%fused_computation.1 | convolution fusion | flops 6444023808 | bytes 14680064 | tf_op jit(solution)/shard_map/dot_general | solution.py:94
  329.1 36.2 %reduce-scatter.5.cloned.1.call-done = bf16[192,2048]{1,0:T(8,128)(2,1)} async-done(((bf16[768,2048]{1,0:T(8,128)(2,1)}), bf16[192,2048]{1,0:T(8,128)(2,1)}) %reduce-scatter.5.cloned.1.call-update) | async-done | bytes 786448 | tf_op jit(solution)/shard_map/reduce_scatter | solution.py:95
  365.3 1.5 fusion.4
  366.9 0.4 multiply_reduce_fusion
  367.4 1.4 add_convert_fusion
  (47 shorter events, 0.8 us)
Async XLA Ops:
  7.4 16.8 %copy-start = (bf16[384,2048]{1,0:T(8,128)(2,1)S(1)}, bf16[384,2048]{1,0:T(8,128)(2,1)}, u32[]{:S(2)}) copy-start(bf16[384,2048]{1,0:T(8,128)(2,1)} %param.15) | copy-start | bytes 4718596
  7.4 8.5 %copy-start.7 = (bf16[768,128]{1,0:T(8,128)(2,1)S(1)}, bf16[768,128]{1,0:T(8,128)(2,1)}, u32[]{:S(2)}) copy-start(bf16[768,128]{1,0:T(8,128)(2,1)} %param.12) | copy-start | bytes 589828
  7.4 8.3 %copy-start.8 = (bf16[768,384]{1,0:T(8,128)(2,1)S(1)}, bf16[768,384]{1,0:T(8,128)(2,1)}, u32[]{:S(2)}) copy-start(bf16[768,384]{1,0:T(8,128)(2,1)} %param.10) | copy-start | bytes 1769476
  7.4 60.5 %reduce-scatter.3.cloned.1.call-start = ((), (), s32[]{:S(2)}) async-start(), calls=%async_computation.2 | async-start | bytes 3932160 | tf_op jit(solution)/shard_map/reduce_scatter | solution.py:84
  8.9 7.1 %collective-permute-start = (bf16[2,128,128]{2,1,0:T(8,128)(2,1)}, bf16[2,128,128]{2,1,0:T(8,128)(2,1)}, u32[]{:S(2)}, u32[]{:S(2)}) collective-permute-start(bf16[2,128,128]{2,1,0:T(8,128)(2,1)} %pad_maximum_fusion.2), channel_id=1, source_target_pairs={{0,4},{4,8},{8,12},{12,16},{16,20},{20,24},{24,28},{1,5},{5,9},{9,... | collective-permute-start | bytes 196616 | tf_op jit(solution)/shard_map/ppermute | solution.py:17
  17.8 1.7 copy-start.11
  19.5 1.4 copy-start.6
  27.7 0.7 copy-start.9
  27.7 0.7 copy-start.10
  27.7 40.1 %copy-start.3 = (bf16[192,2048]{1,0:T(8,128)(2,1)S(1)}, bf16[192,2048]{1,0:T(8,128)(2,1)}, u32[]{:S(2)}) copy-start(bf16[192,2048]{1,0:T(8,128)(2,1)} %param.13) | copy-start | bytes 2359300
  27.8 128.8 %all-gather.9.cloned.1.call-start = ((), (), s32[]{:S(2)}) async-start(), calls=%async_computation.6 | async-start | bytes 9437184 | tf_op jit(solution)/shard_map/all_gather | solution.py:78
  28.3 156.3 %all-gather.5.cloned.1.call-start = ((), (), s32[]{:S(2)}) async-start(), calls=%async_computation.3 | async-start | bytes 3932160 | tf_op jit(solution)/shard_map/all_gather | solution.py:91
  67.8 1.6 copy-start.4
  71.2 239.6 %all-gather.7.cloned.1.call-start = ((), (), s32[]{:S(2)}) async-start(), calls=%async_computation.4 | async-start | bytes 9437184 | tf_op jit(solution)/shard_map/all_gather | solution.py:77
  71.8 293.5 %reduce-scatter.5.cloned.1.call-start = ((), (), s32[]{:S(2)}) async-start(), calls=%async_computation.5 | async-start | bytes 3932160 | tf_op jit(solution)/shard_map/reduce_scatter | solution.py:95
  310.8 10.2 %copy-start.2 = (bf16[2048,8,256]{0,2,1:T(8,128)(2,1)S(1)}, bf16[2048,8,256]{0,2,1:T(8,128)(2,1)}, u32[]{:S(2)}) copy-start(bf16[2048,8,256]{0,2,1:T(8,128)(2,1)} %copy.25) | copy-start | bytes 25165828
  329.1 36.2 %copy-start.1 = (bf16[192,2048]{1,0:T(8,128)(2,1)S(1)}, bf16[192,2048]{1,0:T(8,128)(2,1)}, u32[]{:S(2)}) copy-start(bf16[192,2048]{1,0:T(8,128)(2,1)} %add_convert_fusion.1) | copy-start | bytes 2359300
  365.3 1.6 copy-start.5
Sparse Core Ops, SparseCore 0:
  27.9 39.9 reduce-scatter.2
  329.3 36.0 reduce-scatter.4
Sparse Core Ops, SparseCore 1:
  30.4 126.2 all-gather.8
  158.0 26.5 all-gather.4
  186.6 124.1 all-gather.6
